TPU v7x, 32 devices: a whole 2x2x4 slice. The times are simulated.
32 devices in a mesh: fs: 8 (over z, x), tp: 4 (over y, core).
Axes of the slice: x: 2, y: 2, z: 4, core: 2. Of those that a mesh axis runs over, the one named last changes fastest.
Arguments:
- normed_input: bfloat16 [16384, 2048], P('fs'), may hold values from -6 to 6
- gate_cotangent: bfloat16 [16384, 2048], P('fs', 'tp'), may hold values from -0.125 to 0.125
- first_value_cot: bfloat16 [16384, 1024], P('fs', 'tp'), may hold values from -0.125 to 0.125
- second_value_cot: bfloat16 [16384, 1024], P('fs', 'tp'), may hold values from -0.125 to 0.125
- head_lambda: float32 [8], P('tp'), may hold values from 0.3 to 0.8
- projection: bfloat16 [2048, 256], replicated, may hold values from -1 to 1, as said below
- gate_weight: float32 [2048, 2048], P('fs', 'tp'), may hold values from -0.125 to 0.125
- gate_first: float32 [256, 2048], P('fs', 'tp'), may hold values from -1.5 to 1.5
- gate_second: float32 [256, 2048], P('fs', 'tp'), may hold values from 0.01 to 1
- value_weight: float32 [2048, 1024], P('fs', 'tp'), may hold values from -0.125 to 0.125
- value_first: float32 [256, 1024], P('fs', 'tp'), may hold values from -1.5 to 1.5
- value_second: float32 [256, 1024], P('fs', 'tp'), may hold values from 0.01 to 1
Outputs:
- new_gate_weight: float32 [2048, 2048], P('fs', 'tp')
- gate_step: float32 [2048, 2048], P('fs', 'tp')
- gate_copy: bfloat16 [2048, 2048], P(None, 'tp')
- new_gate_first: float32 [256, 2048], P('fs', 'tp')
- new_gate_second: float32 [256, 2048], P('fs', 'tp')
- new_value_weight: float32 [2048, 1024], P('fs', 'tp')
- value_step: float32 [2048, 1024], P('fs', 'tp')
- value_copy: bfloat16 [2048, 1024], P(None, 'tp')
- new_value_first: float32 [256, 1024], P('fs', 'tp')
- new_value_second: float32 [256, 1024], P('fs', 'tp')
Inputs may be any that keep to these rules, and one draw needn't show every extreme that they name: `projection`: a low-rank factor whose rows differ in scale.
All inputs are finite; a program needn't handle non-finite values.
Results may differ from a plain program's by a relative error of at most 0.0054.
Values may be sent and summed in bfloat16 or wider, within the bound.
A program may use at most 64 MiB of HBM per device.

v0:
```python
import jax
import jax.numpy as jnp
from jax import lax
from jax.sharding import PartitionSpec as P

D = 2048
HEADS = 8
VDIM = 128


moment_decay = 0.9
square_decay = 0.95
adam_floor = 1e-08
learn_rate = 0.02
rms_floor = 0.1


def across_tokens(left, right, precision=None):
    return lax.dot_general(
        left,
        right,
        (((0,), (0,)), ((), ())),
        preferred_element_type=jnp.float32,
        precision=precision,
    )


def moments(first, second, low):
    new_first = moment_decay * first + (1.0 - moment_decay) * low
    new_second = square_decay * second + (1.0 - square_decay) * low * low
    return (new_first, new_second, new_first / (jnp.sqrt(new_second) + adam_floor))


def split_product(stacked, cotangent, factors):
    both = across_tokens(stacked, cotangent)
    return both[:factors] + both[factors:]


def per_device(
    normed_input,
    gate_cotangent,
    first_value_cot,
    second_value_cot,
    head_lambda,
    projection,
    gate_weight,
    gate_first,
    gate_second,
    value_weight,
    value_first,
    value_second,
):
    highest = lax.Precision.HIGHEST
    column_lambda = jnp.repeat(head_lambda, VDIM)
    value_cot = (
        first_value_cot.astype(jnp.float32)
        - column_lambda[None, :] * second_value_cot.astype(jnp.float32)
    ).astype(jnp.bfloat16)
    rows_here = gate_weight.shape[0]
    first_row = lax.axis_index("fs") * rows_here
    local_factor = lax.dynamic_slice_in_dim(projection, first_row, rows_here, 0).astype(jnp.float32)
    projected = jnp.dot(normed_input, projection, preferred_element_type=jnp.float32)
    upper = projected.astype(jnp.bfloat16)
    upper_wide = lax.optimization_barrier(upper).astype(jnp.float32)
    lower = (projected - upper_wide).astype(jnp.bfloat16)
    stacked = jnp.concatenate([upper, lower], axis=1)
    factors = projection.shape[1]
    partial_gate = split_product(stacked, gate_cotangent, factors)
    partial_value = split_product(stacked, value_cot, factors)
    gate_low, value_low = (
        lax.psum_scatter(partial_gate, "fs", scatter_dimension=0, tiled=True),
        lax.psum_scatter(partial_value, "fs", scatter_dimension=0, tiled=True),
    )
    new_gate_first, new_gate_second, gate_dir = moments(gate_first, gate_second, gate_low)
    new_value_first, new_value_second, value_dir = moments(value_first, value_second, value_low)
    gate_update = jnp.dot(
        local_factor, lax.all_gather(gate_dir, "fs", axis=0, tiled=True), precision=highest
    )
    value_update = jnp.dot(
        local_factor, lax.all_gather(value_dir, "fs", axis=0, tiled=True), precision=highest
    )
    gate_total, value_total = lax.psum(
        (jnp.sum(gate_update * gate_update), jnp.sum(value_update * value_update)), ("fs", "tp")
    )
    gate_step = gate_update / (jnp.sqrt(gate_total / (D * D)) + rms_floor)
    value_step = value_update / (jnp.sqrt(value_total / (D * HEADS * VDIM)) + rms_floor)
    new_gate_weight = gate_weight - learn_rate * gate_step
    new_value_weight = value_weight - learn_rate * value_step
    gate_copy, value_copy = (
        lax.all_gather(new_gate_weight.astype(jnp.bfloat16), "fs", axis=0, tiled=True),
        lax.all_gather(new_value_weight.astype(jnp.bfloat16), "fs", axis=0, tiled=True),
    )
    return (
        new_gate_weight,
        gate_step,
        gate_copy,
        new_gate_first,
        new_gate_second,
        new_value_weight,
        value_step,
        value_copy,
        new_value_first,
        new_value_second,
    )


def solution(mesh):
    placed = (
        P("fs", None),
        P("fs", "tp"),
        P("fs", "tp"),
        P("fs", "tp"),
        P("tp"),
        P(),
        P("fs", "tp"),
        P("fs", "tp"),
        P("fs", "tp"),
        P("fs", "tp"),
        P("fs", "tp"),
        P("fs", "tp"),
    )
    return jax.shard_map(
        per_device,
        mesh=mesh,
        in_specs=placed,
        out_specs=(
            P("fs", "tp"),
            P("fs", "tp"),
            P(None, "tp"),
            P("fs", "tp"),
            P("fs", "tp"),
            P("fs", "tp"),
            P("fs", "tp"),
            P(None, "tp"),
            P("fs", "tp"),
            P("fs", "tp"),
        ),
        check_vma=False,
    )
```

profile of v0, /device:TPU:12, one launch (start us, length us, event | category | flops | bytes accessed | tf_op | source)
XLA Modules:
  0.0 323.4 jit_solution(1942997298936797233)
XLA Ops:
  7.2 6.1 %fusion.17 = (bf16[2048,256]{0,1:T(8,128)(2,1)S(1)}, f32[2048,256]{0,1:T(8,128)S(1)}) fusion(bf16[2048,2048]{1,0:T(8,128)(2,1)} %param.12, bf16[2048,256]{1,0:T(8,128)(2,1)} %param.17), kind=kOutput, calls=%fused_computation.33 | convolution fusion | flops 2148007936 | bytes 12582912 | tf_op jit(solution)/shard_map/dot_general | solution.py:62
  13.5 0.3 subtract_convert_fusion.1
  13.7 0.9 copy-done.8
  14.7 0.3 copy-done.9
  15.0 0.8 fusion
  15.8 0.2 copy-done.2
  16.0 0.7 slice_add_fusion.1
  16.8 2.5 fusion.1
  19.3 0.9 slice_add_fusion
  20.3 59.8 %reduce-scatter.5.cloned.1.call-done = f32[32,256]{1,0:T(8,128)} async-done(((f32[256,256]{1,0:T(8,128)}), f32[32,256]{1,0:T(8,128)}) %reduce-scatter.5.cloned.1.call-update) | async-done | bytes 32784 | tf_op jit(solution)/shard_map/reduce_scatter | solution.py:72
  80.1 1.4 add_divide_fusion.1
  81.4 28.4 %all_gather.14 = f32[256,256]{1,0:T(8,128)S(1)} all-gather(f32[32,256]{1,0:T(8,128)S(1)} %get-tuple-element.18), channel_id=1, replica_groups=mesh['fs'=8,'tp'=4] {'fs'}, dimensions={0}, use_global_device_ids=true | all-gather | bytes 294912 | tf_op jit(solution)/shard_map/all_gather | solution.py:80
  109.9 1.9 multiply_reduce_fusion.1
  111.7 33.9 %reduce-scatter.3.cloned.1.call-done = f32[32,512]{1,0:T(8,128)} async-done(((f32[256,512]{1,0:T(8,128)}), f32[32,512]{1,0:T(8,128)}) %reduce-scatter.3.cloned.1.call-update) | async-done | bytes 65552 | tf_op jit(solution)/shard_map/reduce_scatter | solution.py:71
  145.7 1.5 add_divide_fusion
  147.2 28.8 %all_gather.12 = f32[256,512]{1,0:T(8,128)S(1)} all-gather(f32[32,512]{1,0:T(8,128)S(1)} %get-tuple-element.21), channel_id=1, replica_groups=mesh['fs'=8,'tp'=4] {'fs'}, dimensions={0}, use_global_device_ids=true | all-gather | bytes 589824 | tf_op jit(solution)/shard_map/all_gather | solution.py:77
  176.0 2.0 multiply_reduce_fusion
  178.0 42.2 %all-reduce = (f32[]{:T(128)}, f32[]{:T(128)}) all-reduce(f32[]{:T(128)} %get-tuple-element.26, f32[]{:T(128)} %get-tuple-element.28), channel_id=1, replica_groups=mesh['fs'=8,'tp'=4] {'fs','tp'}, use_global_device_ids=true, to_apply=%region_2.0 | all-reduce | flops 2 | bytes 16 | tf_op jit(solution)/shard_map/psum | solution.py:82
  220.9 1.8 fusion.13
  223.5 1.2 fusion.14
  224.8 36.4 %all-gather.5.cloned.1.call-done = bf16[2048,256]{1,0:T(8,128)(2,1)} async-done(((bf16[256,256]{1,0:T(8,128)(2,1)}), bf16[2048,256]{1,0:T(8,128)(2,1)}) %all-gather.5.cloned.1.call-update) | async-done | bytes 1048592 | tf_op jit(solution)/shard_map/all_gather | solution.py:91
  261.2 51.6 %all-gather.3.cloned.1.call-done = bf16[2048,512]{1,0:T(8,128)(2,1)} async-done(((bf16[256,512]{1,0:T(8,128)(2,1)}), bf16[2048,512]{1,0:T(8,128)(2,1)}) %all-gather.3.cloned.1.call-update) | async-done | bytes 2097168 | tf_op jit(solution)/shard_map/all_gather | solution.py:90
  312.8 3.1 copy.24
  315.9 1.0 copy.25
  (28 shorter events, 0.4 us)
Async XLA Ops:
  7.2 9.6 %copy-start = (bf16[2048,512]{1,0:T(8,128)(2,1)S(1)}, bf16[2048,512]{1,0:T(8,128)(2,1)}, u32[]{:S(2)}) copy-start(bf16[2048,512]{1,0:T(8,128)(2,1)} %param.13) | copy-start | bytes 6291460
  7.2 6.2 %copy-start.10 = (f32[2]{0:T(128)S(1)}, f32[2]{0:T(128)}, u32[]{:S(2)}) copy-start(f32[2]{0:T(128)} %param.16) | copy-start | bytes 28
  7.2 72.8 %reduce-scatter.5.cloned.1.call-start = ((), (), s32[]{:S(2)}) async-start(), calls=%async_computation.4 | async-start | bytes 294912 | tf_op jit(solution)/shard_map/reduce_scatter | solution.py:72
  13.5 1.2 copy-start.8
  13.5 1.5 copy-start.9
  15.0 1.0 copy-start.2
  16.7 128.9 %reduce-scatter.3.cloned.1.call-start = ((), (), s32[]{:S(2)}) async-start(), calls=%async_computation.2 | async-start | bytes 589824 | tf_op jit(solution)/shard_map/reduce_scatter | solution.py:71
  19.3 60.8 %copy-start.6 = (f32[32,256]{1,0:T(8,128)S(1)}, f32[32,256]{1,0:T(8,128)}, u32[]{:S(2)}) copy-start(f32[32,256]{1,0:T(8,128)} %param.23) | copy-start | bytes 98308
  19.3 60.8 %copy-start.7 = (f32[32,256]{1,0:T(8,128)S(1)}, f32[32,256]{1,0:T(8,128)}, u32[]{:S(2)}) copy-start(f32[32,256]{1,0:T(8,128)} %param.22) | copy-start | bytes 98308
  19.3 126.4 %copy-start.4 = (f32[32,512]{1,0:T(8,128)S(1)}, f32[32,512]{1,0:T(8,128)}, u32[]{:S(2)}) copy-start(f32[32,512]{1,0:T(8,128)} %param.20) | copy-start | bytes 196612
  19.3 126.4 %copy-start.5 = (f32[32,512]{1,0:T(8,128)S(1)}, f32[32,512]{1,0:T(8,128)}, u32[]{:S(2)}) copy-start(f32[32,512]{1,0:T(8,128)} %param.19) | copy-start | bytes 196612
  20.2 241.0 %all-gather.5.cloned.1.call-start = ((), (), s32[]{:S(2)}) async-start(), calls=%async_computation.5 | async-start | bytes 1179648 | tf_op jit(solution)/shard_map/all_gather | solution.py:91
  109.9 113.7 %copy-start.3 = (f32[256,512]{1,0:T(8,128)S(1)}, f32[256,512]{1,0:T(8,128)}, u32[]{:S(2)}) copy-start(f32[256,512]{1,0:T(8,128)} %param.18) | copy-start | bytes 1572868
  222.8 90.0 %all-gather.3.cloned.1.call-start = ((), (), s32[]{:S(2)}) async-start(), calls=%async_computation.3 | async-start | bytes 2359296 | tf_op jit(solution)/shard_map/all_gather | solution.py:90
  312.8 3.1 copy-start.1
Sparse Core Ops, SparseCore 0:
  16.8 63.1 reduce-scatter.4
  84.0 61.6 reduce-scatter.2
  222.9 38.2 all-gather.4
  263.7 48.9 all-gather.2
where the time goes:
time: 325 us; the launch traced here: 323 us
  waiting for transfers between devices  182 us (56%)
  blocking collectives  99.4 us (31%)
  between operations  15.3 us (5%)
  matrix products  13.3 us (4%)
  other arithmetic  7.83 us (2%)
  local copies, waits for them, and re-layouts  5.67 us (2%)
    reduce_scatter x1, waiting for transfers between devices, per_device(): lax.psum_scatter(partial_value, 'fs', scatter_dimension=0, tiled=True)  59.8 us
    all_gather x1, waiting for transfers between devices, per_device(): lax.all_gather(new_gate_weight.astype(jnp.bfloat16), 'fs', axis=0, tiled=...  51.6 us
    psum x1, blocking collectives, per_device(): lax.psum((jnp.sum(gate_update * gate_update), jnp.sum(value_update * valu...  42.2 us
    all_gather x1, waiting for transfers between devices, per_device(): lax.all_gather(new_value_weight.astype(jnp.bfloat16), 'fs', axis=0, tiled...  36.4 us
    reduce_scatter x1, waiting for transfers between devices, per_device(): lax.psum_scatter(partial_gate, 'fs', scatter_dimension=0, tiled=True)  33.9 us
    all_gather x1, blocking collectives, per_device(): lax.all_gather(gate_dir, 'fs', axis=0, tiled=True)  28.8 us
    all_gather x1, blocking collectives, per_device(): lax.all_gather(value_dir, 'fs', axis=0, tiled=True)  28.4 us
  transfers between devices with their start and end apart: 4, of which 4 were waited for; matrix products, arithmetic and copies ran while one was open for 2% of the time, Pallas kernels for 0%

commit v1 on v0

v1 whole, which is shorter than its diff:
```python
import functools

import jax
import jax.numpy as jnp
from jax import lax
from jax.experimental import pallas as pl
from jax.experimental.pallas import tpu as pltpu
from jax.sharding import PartitionSpec as P

VDIM = 128
PIECES = 4
CHUNKS = 4
STEP_TOKENS = 256

moment_decay = 0.9
square_decay = 0.95
adam_floor = 1e-08
learn_rate = 0.02
rms_floor = 0.1

MESH = pl.DeviceIdType.MESH
f32, bf16 = jnp.float32, jnp.bfloat16


def factor_fs(count):
    inner = 1
    while (2 * inner) ** 2 <= count and count % (2 * inner) == 0:
        inner *= 2
    return count // inner, inner


def kernel(
    nz,
    nx,
    nt,
    x_hbm,
    gcot_hbm,
    fcot_hbm,
    scot_hbm,
    lam_ref,
    proj_hbm,
    gw_hbm,
    gm_hbm,
    gs_hbm,
    vw_hbm,
    vm_hbm,
    vs_hbm,
    ngw_hbm,
    gstep_hbm,
    gcopy_hbm,
    ngm_hbm,
    ngs_hbm,
    nvw_hbm,
    vstep_hbm,
    vcopy_hbm,
    nvm_hbm,
    nvs_hbm,
    xv,
    gcv,
    fcv,
    scv,
    pv,
    gw,
    vw,
    gm,
    gs,
    vm,
    vs,
    wall,
    acc,
    rsrc,
    rsx,
    zsrc,
    rsz,
    dall,
    dcat,
    upd,
    sums,
    gcs,
    vcs,
    gsteps,
    vsteps,
    in_sem,
    x_sem,
    out_sem,
    copy_sem,
    wz_send,
    wz_recv,
    wx_send,
    wx_recv,
    rx_send,
    rx_recv,
    rz_send,
    rz_recv,
    dz_send,
    dz_recv,
    dx_send,
    dx_recv,
    t_send,
    t_recv,
):
    nfs = nz * nx
    f = lax.axis_index("fs")
    t = lax.axis_index("tp")
    z = lax.div(f, nx)
    x = lax.rem(f, nx)
    rows, cg = gw.shape
    cv = vw.shape[1]
    cols = cg + cv
    rank = acc.shape[0]
    share = rank // nfs
    part = rows // PIECES
    tokens = x_hbm.shape[0] // CHUNKS

    def zpeer(k):
        return lax.rem(z + k, nz)

    def xpeer(k):
        return lax.rem(x + k, nx)

    barrier = pltpu.get_barrier_semaphore()
    for k in range(1, nz):
        pl.semaphore_signal(barrier, inc=1, device_id=(zpeer(k) * nx + x, t), device_id_type=MESH)
    for k in range(1, nx):
        pl.semaphore_signal(barrier, inc=1, device_id=(z * nx + xpeer(k), t), device_id_type=MESH)
    for k in range(1, nt):
        pl.semaphore_signal(barrier, inc=1, device_id=(f, lax.rem(t + k, nt)), device_id_type=MESH)

    small = [
        pltpu.make_async_copy(src, dst, in_sem.at[i])
        for i, (src, dst) in enumerate(
            [
                (gw_hbm, gw),
                (vw_hbm, vw),
                (proj_hbm, pv),
                (gm_hbm, gm),
                (gs_hbm, gs),
                (vm_hbm, vm),
                (vs_hbm, vs),
            ]
        )
    ]

    def chunk_copies(c):
        at = pl.ds(c * tokens, tokens)
        return [
            pltpu.make_async_copy(src.at[at], dst.at[at], x_sem.at[i, c])
            for i, (src, dst) in enumerate(
                [(x_hbm, xv), (gcot_hbm, gcv), (fcot_hbm, fcv), (scot_hbm, scv)]
            )
        ]

    for i in range(3):
        small[i].start()
    for c in range(CHUNKS):
        for copy in chunk_copies(c):
            copy.start()
    for i in range(3, 7):
        small[i].start()

    small[0].wait()
    small[1].wait()
    for p in range(PIECES):
        at = pl.ds(p * part, part)
        wall[f, p, :, :cg] = gw[at, :].astype(bf16)
        wall[f, p, :, cg:] = vw[at, :].astype(bf16)

    def wz(k, p, src_z):
        owner = src_z * nx + x
        return pltpu.make_async_remote_copy(
            src_ref=wall.at[owner, p],
            dst_ref=wall.at[owner, p],
            send_sem=wz_send.at[k, p],
            recv_sem=wz_recv.at[src_z, p],
            device_id=(zpeer(k) * nx + x, t),
            device_id_type=MESH,
        )

    def wx(k, p, src_z, src_x):
        owner = src_z * nx + src_x
        return pltpu.make_async_remote_copy(
            src_ref=wall.at[owner, p],
            dst_ref=wall.at[owner, p],
            send_sem=wx_send.at[k, src_z, p],
            recv_sem=wx_recv.at[src_x, src_z, p],
            device_id=(z * nx + xpeer(k), t),
            device_id_type=MESH,
        )

    def send_z(p):
        for k in range(1, nz):
            wz(k, p, z).start()

    def relay(p):
        for k in range(1, nz):
            wz(k, p, zpeer(k)).wait_recv()
            for m in range(1, nx):
                wx(m, p, zpeer(k), x).start()

    pl.semaphore_wait(barrier, (nz - 1) + (nx - 1) + (nt - 1))
    send_z(0)
    for p in range(PIECES):
        for k in range(1, nx):
            wx(k, p, z, x).start()

    small[2].wait()
    acc[...] = jnp.zeros_like(acc)
    for c in range(CHUNKS):
        for copy in chunk_copies(c):
            copy.wait()

        def multiply(i, carry):
            at = pl.ds(pl.multiple_of(c * tokens + i * STEP_TOKENS, STEP_TOKENS), STEP_TOKENS)
            upper = jnp.dot(xv[at, :], pv[...], preferred_element_type=f32).astype(bf16)
            lam = lam_ref[...]
            value = (fcv[at, :].astype(f32) - lam * scv[at, :].astype(f32)).astype(bf16)
            over = (((0,), (0,)), ((), ()))
            acc[:, :cg] += lax.dot_general(upper, gcv[at, :], over, preferred_element_type=f32)
            acc[:, cg:] += lax.dot_general(upper, value, over, preferred_element_type=f32)
            return carry

        lax.fori_loop(0, tokens // STEP_TOKENS, multiply, 0)

    for zi in range(nz):
        for xi in range(nx):
            at = pl.ds((zi * nx + xi) * share, share)
            rsrc[xi, zi] = acc[at, :].astype(bf16)

    def rx(k, src_x, dst_x):
        return pltpu.make_async_remote_copy(
            src_ref=rsrc.at[dst_x],
            dst_ref=rsx.at[src_x],
            send_sem=rx_send.at[k],
            recv_sem=rx_recv.at[src_x],
            device_id=(z * nx + xpeer(k), t),
            device_id_type=MESH,
        )

    for k in range(1, nx):
        rx(k, x, xpeer(k)).start()
    send_z(1)
    relay(0)
    for k in range(1, nx):
        rx(k, xpeer(k), x).wait_recv()
    for zi in range(nz):
        at = pl.ds(pl.multiple_of((zi * nx + x) * share, share), share)
        total = acc[at, :]
        for k in range(1, nx):
            total = total + rsx[xpeer(k), zi].astype(f32)
        zsrc[zi] = total.astype(bf16)

    def rz(k, src_z, dst_z):
        return pltpu.make_async_remote_copy(
            src_ref=zsrc.at[dst_z],
            dst_ref=rsz.at[src_z],
            send_sem=rz_send.at[k],
            recv_sem=rz_recv.at[src_z],
            device_id=(zpeer(k) * nx + x, t),
            device_id_type=MESH,
        )

    for k in range(1, nz):
        rz(k, z, zpeer(k)).start()
    send_z(2)
    relay(1)
    for i in range(3, 7):
        small[i].wait()
    low = zsrc[z].astype(f32)
    for k in range(1, nz):
        rz(k, zpeer(k), z).wait_recv()
        low = low + rsz[zpeer(k)].astype(f32)

    for first, second, at in ((gm, gs, slice(0, cg)), (vm, vs, slice(cg, cols))):
        mine = low[:, at]
        new_first = moment_decay * first[...] + (1.0 - moment_decay) * mine
        new_second = square_decay * second[...] + (1.0 - square_decay) * mine * mine
        first[...] = new_first
        second[...] = new_second
        dall[f, :, at] = (new_first / (jnp.sqrt(new_second) + adam_floor)).astype(bf16)

    outs = [
        pltpu.make_async_copy(src, dst, out_sem.at[i])
        for i, (src, dst) in enumerate(
            [
                (gm, ngm_hbm),
                (gs, ngs_hbm),
                (vm, nvm_hbm),
                (vs, nvs_hbm),
                (gw, ngw_hbm),
                (vw, nvw_hbm),
                (gsteps, gstep_hbm),
                (vsteps, vstep_hbm),
            ]
        )
    ]
    for i in range(4):
        outs[i].start()

    def dz(k, src_z):
        owner = src_z * nx + x
        return pltpu.make_async_remote_copy(
            src_ref=dall.at[owner],
            dst_ref=dall.at[owner],
            send_sem=dz_send.at[k],
            recv_sem=dz_recv.at[src_z],
            device_id=(zpeer(k) * nx + x, t),
            device_id_type=MESH,
        )

    def dx(k, src_z, src_x):
        owner = src_z * nx + src_x
        return pltpu.make_async_remote_copy(
            src_ref=dall.at[owner],
            dst_ref=dall.at[owner],
            send_sem=dx_send.at[k, src_z],
            recv_sem=dx_recv.at[src_x, src_z],
            device_id=(z * nx + xpeer(k), t),
            device_id_type=MESH,
        )

    for k in range(1, nz):
        dz(k, z).start()
    for m in range(1, nx):
        dx(m, z, x).start()
    send_z(3)
    relay(2)
    for k in range(1, nz):
        dz(k, zpeer(k)).wait_recv()
        for m in range(1, nx):
            dx(m, zpeer(k), x).start()
    for m in range(1, nx):
        for zi in range(nz):
            dx(m, zi, xpeer(m)).wait_recv()

    for j in range(nfs):
        dcat[pl.ds(j * share, share), :] = dall[j].astype(f32)
    direction = dcat[...].astype(bf16)

    def expand(j, squares):
        left = pv[pl.ds(pl.multiple_of(j * rows, rows), rows), :]
        block = jnp.dot(left, direction, preferred_element_type=f32)
        upd[j] = block
        return squares + jnp.sum(block * block, axis=0, keepdims=True)

    squares = lax.fori_loop(0, nfs, expand, jnp.zeros((1, cols), f32))
    gate_sum = jnp.sum(squares[:, :cg], axis=1, keepdims=True)
    value_sum = jnp.sum(squares[:, cg:], axis=1, keepdims=True)
    sums[t, 0] = jnp.broadcast_to(gate_sum, (8, 128))
    sums[t, 1] = jnp.broadcast_to(value_sum, (8, 128))

    def tp(k, src_t):
        return pltpu.make_async_remote_copy(
            src_ref=sums.at[src_t],
            dst_ref=sums.at[src_t],
            send_sem=t_send.at[k],
            recv_sem=t_recv.at[src_t],
            device_id=(f, lax.rem(t + k, nt)),
            device_id_type=MESH,
        )

    for k in range(1, nt):
        tp(k, t).start()
    relay(3)
    for k in range(1, nt):
        tp(k, lax.rem(t + k, nt)).wait_recv()
    whole = sums[0]
    for k in range(1, nt):
        whole = whole + sums[k]
    entries = nfs * rows * nt
    gscale = (1.0 / (jnp.sqrt(whole[0] / (entries * cg)) + rms_floor))[0:1, 0:1]
    vscale = (1.0 / (jnp.sqrt(whole[1] / (entries * cv)) + rms_floor))[0:1, 0:1]

    gstep = upd[f, :, :cg] * gscale
    vstep = upd[f, :, cg:] * vscale
    gsteps[...] = gstep
    vsteps[...] = vstep
    gw[...] = gw[...] - learn_rate * gstep
    vw[...] = vw[...] - learn_rate * vstep
    for i in range(4, 8):
        outs[i].start()

    copies = []
    for p in range(PIECES):
        for m in range(1, nx):
            for zi in range(nz):
                wx(m, p, zi, xpeer(m)).wait_recv()
        at = pl.ds(p * part, part)

        def finish(j, carry):
            gcs[j, p] = (wall[j, p, :, :cg].astype(f32) - learn_rate * (upd[j, at, :cg] * gscale)).astype(bf16)
            vcs[j, p] = (wall[j, p, :, cg:].astype(f32) - learn_rate * (upd[j, at, cg:] * vscale)).astype(bf16)
            return carry

        lax.fori_loop(0, nfs, finish, 0)
        for i, (src, dst) in enumerate([(gcs, gcopy_hbm), (vcs, vcopy_hbm)]):
            copies.append(pltpu.make_async_copy(src.at[:, p], dst.at[:, p], copy_sem.at[i, p]))
            copies[-1].start()

    for copy in copies + outs:
        copy.wait()
    for k in range(1, nz):
        for p in range(PIECES):
            wz(k, p, z).wait_send()
        rz(k, z, zpeer(k)).wait_send()
        dz(k, z).wait_send()
    for m in range(1, nx):
        rx(m, x, xpeer(m)).wait_send()
        for zi in range(nz):
            for p in range(PIECES):
                wx(m, p, zi, x).wait_send()
            dx(m, zi, x).wait_send()
    for k in range(1, nt):
        tp(k, t).wait_send()


def per_device(nz, nx, nt, xin, gcot, fcot, scot, lam, proj, gw, gm, gs, vw, vm, vs):
    nfs = nz * nx
    rows, cg = gw.shape
    cv = vw.shape[1]
    cols = cg + cv
    depth, rank = proj.shape
    share = rank // nfs
    part = rows // PIECES
    column_lambda = jnp.repeat(lam, VDIM)[None, :]
    anywhere = pl.BlockSpec(memory_space=pl.ANY)
    dma = pltpu.SemaphoreType.DMA
    shape = jax.ShapeDtypeStruct
    like = lambda a: shape(a.shape, a.dtype)
    results = pl.pallas_call(
        functools.partial(kernel, nz, nx, nt),
        out_shape=[
            like(gw),
            like(gw),
            shape((nfs, PIECES, part, cg), bf16),
            like(gm),
            like(gs),
            like(vw),
            like(vw),
            shape((nfs, PIECES, part, cv), bf16),
            like(vm),
            like(vs),
        ],
        in_specs=[anywhere] * 4 + [pl.BlockSpec(memory_space=pltpu.VMEM)] + [anywhere] * 7,
        out_specs=[anywhere] * 10,
        scratch_shapes=[
            pltpu.VMEM(xin.shape, bf16),
            pltpu.VMEM(gcot.shape, bf16),
            pltpu.VMEM(fcot.shape, bf16),
            pltpu.VMEM(scot.shape, bf16),
            pltpu.VMEM(proj.shape, bf16),
            pltpu.VMEM(gw.shape, f32),
            pltpu.VMEM(vw.shape, f32),
            pltpu.VMEM(gm.shape, f32),
            pltpu.VMEM(gs.shape, f32),
            pltpu.VMEM(vm.shape, f32),
            pltpu.VMEM(vs.shape, f32),
            pltpu.VMEM((nfs, PIECES, part, cols), bf16),
            pltpu.VMEM((rank, cols), f32),
            pltpu.VMEM((nx, nz, share, cols), bf16),
            pltpu.VMEM((nx, nz, share, cols), bf16),
            pltpu.VMEM((nz, share, cols), bf16),
            pltpu.VMEM((nz, share, cols), bf16),
            pltpu.VMEM((nfs, share, cols), bf16),
            pltpu.VMEM((rank, cols), f32),
            pltpu.VMEM((nfs, rows, cols), f32),
            pltpu.VMEM((nt, 2, 8, 128), f32),
            pltpu.VMEM((nfs, PIECES, part, cg), bf16),
            pltpu.VMEM((nfs, PIECES, part, cv), bf16),
            pltpu.VMEM(gw.shape, f32),
            pltpu.VMEM(vw.shape, f32),
            dma((7,)),
            dma((4, CHUNKS)),
            dma((8,)),
            dma((2, PIECES)),
            dma((nz, PIECES)),
            dma((nz, PIECES)),
            dma((nx, nz, PIECES)),
            dma((nx, nz, PIECES)),
            dma((nx,)),
            dma((nx,)),
            dma((nz,)),
            dma((nz,)),
            dma((nz,)),
            dma((nz,)),
            dma((nx, nz)),
            dma((nx, nz)),
            dma((nt,)),
            dma((nt,)),
        ],
        compiler_params=pltpu.CompilerParams(
            collective_id=0, has_side_effects=True, vmem_limit_bytes=60 * 1024 * 1024
        ),
    )(xin, gcot, fcot, scot, column_lambda, proj, gw, gm, gs, vw, vm, vs)
    results = list(results)
    results[2] = results[2].reshape(depth, cg)
    results[7] = results[7].reshape(depth, cv)
    return tuple(results)


def solution(mesh):
    nz, nx = factor_fs(mesh.shape["fs"])
    split, whole = P("fs", "tp"), P(None, "tp")
    placed = (P("fs", None), split, split, split, P("tp"), P()) + (split,) * 6
    return jax.shard_map(
        functools.partial(per_device, nz, nx, mesh.shape["tp"]),
        mesh=mesh,
        in_specs=placed,
        out_specs=(split, split, whole, split, split, split, split, whole, split, split),
        check_vma=False,
    )
```

time: 325 us -> 77.3 us (0.24)
  waiting for transfers between devices: 182 us -> 0 us
  blocking collectives: 99.4 us -> 0 us
  Pallas kernels: 0 us -> 65 us
  between operations: 15.3 us -> 0.69 us
  matrix products: 13.3 us -> 0 us
  other arithmetic: 7.83 us -> 0 us
  local copies, waits for them, and re-layouts: 5.67 us -> 11.4 us
    reduce_scatter x2 -> x0, waiting for transfers between devices: 93.7 us -> none  [the longest x1 59.8 us: per_device(): lax.psum_scatter(partial_value, 'fs', scatter_dimension=0, tiled=True)]
    all_gather x2 -> x0, waiting for transfers between devices: 88 us -> none  [the longest x1 51.6 us: per_device(): lax.all_gather(new_gate_weight.astype(jnp.bfloat16), 'fs', axis=0, tiled=...]
    pallas_call x0 -> x1, Pallas kernels: none -> 65 us  [per_device(): pl.pallas_call(functools.partial(kernel, nz, nx, nt), out_shape=[like(gw)...]
    all_gather x2 -> x0, blocking collectives: 57.2 us -> none  [the longest x1 28.8 us: per_device(): lax.all_gather(gate_dir, 'fs', axis=0, tiled=True)]
    psum x1 -> x0, blocking collectives: 42.2 us -> none  [per_device(): lax.psum((jnp.sum(gate_update * gate_update), jnp.sum(value_update * valu...]
    dot_general x5 -> x0, matrix products: 13.3 us -> none  [the longest x1 6.12 us: per_device(): jnp.dot(normed_input, projection, preferred_element_type=jnp.float32)]
    unnamed x24 -> x26, local copies, waits for them, and re-layouts: 5.6 us -> 10.1 us
    convert_element_type x3 -> x0, other arithmetic: 3.31 us -> none  [the longest x1 1.83 us: per_device(): new_value_weight.astype(jnp.bfloat16)]
  transfers between devices with their start and end apart: 4 -> 0, of which waited for: 4 -> 0; matrix products, arithmetic and copies ran while one was open for 2% -> 0% of each run, Pallas kernels for 0% -> 0%
where the time goes in v1:
time: 77.3 us; the launch traced here: 77.1 us
  Pallas kernels  65 us (84%)
  local copies, waits for them, and re-layouts  11.4 us (15%)
    pallas_call x1, Pallas kernels, per_device(): pl.pallas_call(functools.partial(kernel, nz, nx, nt), out_shape=[like(gw)...  65 us
    unnamed x26, local copies, waits for them, and re-layouts  10.1 us

profile of v1, /device:TPU:12, one launch (start us, length us, event | category | flops | bytes accessed | tf_op | source)
XLA Modules:
  0.0 77.1 jit_solution(14929575527372971370)
XLA Ops:
  0.6 1.3 %broadcast_in_dim.3 = f32[2,128]{1,0:T(2,128)} broadcast(f32[2]{0:T(128)} %param.16), dimensions={0} | broadcast | bytes 1032 | tf_op jit(solution)/shard_map/broadcast_in_dim | solution.py:424
  1.9 65.0 %shard_map.195 = (f32[256,512]{1,0:T(8,128)}, f32[256,512]{1,0:T(8,128)}, bf16[8,4,64,512]{3,2,1,0:T(8,128)(2,1)}, f32[32,512]{1,0:T(8,128)}, f32[32,512]{1,0:T(...) custom-call(bf16[2048,2048]{1,0:T(8,128)(2,1)} %x_hbm.1, ...), custom_call_target="tpu_custom_call" | custom-call | tf_op jit(solution)/shard_map/pallas_call | solution.py:429
  66.9 0.0 copy-start
  66.9 2.0 %copy.32 = f32[256,512]{1,0:T(8,128)} copy(f32[256,512]{1,0:T(8,128)} %get-tuple-element.40) | data formatting | bytes 1048576
  68.9 1.9 %copy.33 = f32[256,512]{1,0:T(8,128)} copy(f32[256,512]{1,0:T(8,128)} %get-tuple-element.41) | data formatting | bytes 1048576
  70.8 0.0 copy-done
  70.8 0.0 copy-start.5
  70.8 0.0 copy-start.2
  70.8 0.0 copy-start.1
  70.8 1.3 %copy.34 = bf16[2048,512]{1,0:T(8,128)(2,1)} copy(bf16[2048,512]{1,0:T(8,128)(2,1)S(1)} %bitcast.3) | data formatting | bytes 4194304
  72.2 0.0 copy-done.5
  72.2 0.6 copy.35
  72.8 0.0 copy-done.4
  72.8 0.6 copy.36
  73.4 0.0 copy-done.3
  73.4 0.7 copy.37
  74.1 0.0 copy-done.2
  74.1 0.7 copy.38
  74.8 0.0 copy-done.1
  74.8 1.0 %copy.39 = bf16[2048,256]{1,0:T(8,128)(2,1)} copy(bf16[2048,256]{1,0:T(8,128)(2,1)S(1)} %bitcast.4) | data formatting | bytes 2097152
  75.8 0.0 copy-done.7
  75.8 0.6 copy.40
  76.4 0.0 copy-done.6
  76.4 0.6 copy.41
  (4 shorter events, 0.0 us)
Async XLA Ops:
  66.9 3.9 %copy-start = (bf16[8,4,64,512]{3,2,1,0:T(8,128)(2,1)S(1)}, bf16[8,4,64,512]{3,2,1,0:T(8,128)(2,1)}, u32[]{:S(2)}) copy-start(bf16[8,4,64,512]{3,2,1,0:T(8,128)(2,1)} %get-tuple-element.22) | copy-start | bytes 6291460
  70.8 1.4 %copy-start.5 = (f32[32,512]{1,0:T(8,128)S(1)}, f32[32,512]{1,0:T(8,128)}, u32[]{:S(2)}) copy-start(f32[32,512]{1,0:T(8,128)} %get-tuple-element.43) | copy-start | bytes 196612
  70.8 2.0 %copy-start.4 = (f32[32,512]{1,0:T(8,128)S(1)}, f32[32,512]{1,0:T(8,128)}, u32[]{:S(2)}) copy-start(f32[32,512]{1,0:T(8,128)} %get-tuple-element.44) | copy-start | bytes 196612
  70.8 2.6 %copy-start.3 = (f32[256,256]{1,0:T(8,128)S(1)}, f32[256,256]{1,0:T(8,128)}, u32[]{:S(2)}) copy-start(f32[256,256]{1,0:T(8,128)} %get-tuple-element.45) | copy-start | bytes 786436
  70.8 3.3 %copy-start.2 = (f32[256,256]{1,0:T(8,128)S(1)}, f32[256,256]{1,0:T(8,128)}, u32[]{:S(2)}) copy-start(f32[256,256]{1,0:T(8,128)} %get-tuple-element.46) | copy-start | bytes 786436
  70.8 4.0 %copy-start.1 = (bf16[8,4,64,256]{3,2,1,0:T(8,128)(2,1)S(1)}, bf16[8,4,64,256]{3,2,1,0:T(8,128)(2,1)}, u32[]{:S(2)}) copy-start(bf16[8,4,64,256]{3,2,1,0:T(8,128)(2,1)} %get-tuple-element.27) | copy-start | bytes 3145732
  72.2 3.7 %copy-start.7 = (f32[32,256]{1,0:T(8,128)S(1)}, f32[32,256]{1,0:T(8,128)}, u32[]{:S(2)}) copy-start(f32[32,256]{1,0:T(8,128)} %get-tuple-element.48) | copy-start | bytes 98308
  72.2 4.3 %copy-start.6 = (f32[32,256]{1,0:T(8,128)S(1)}, f32[32,256]{1,0:T(8,128)}, u32[]{:S(2)}) copy-start(f32[32,256]{1,0:T(8,128)} %get-tuple-element.49) | copy-start | bytes 98308

commit v2 on v1

--- a/solution.py
+++ b/solution.py
@@ -45,14 +45,11 @@
     vw_hbm,
     vm_hbm,
     vs_hbm,
-    ngw_hbm,
-    gstep_hbm,
-    gcopy_hbm,
+    wall_hbm,
+    dir_hbm,
+    scale_hbm,
     ngm_hbm,
     ngs_hbm,
-    nvw_hbm,
-    vstep_hbm,
-    vcopy_hbm,
     nvm_hbm,
     nvs_hbm,
     xv,
@@ -74,12 +71,9 @@
     rsz,
     dall,
     dcat,
-    upd,
+    direct,
     sums,
-    gcs,
-    vcs,
-    gsteps,
-    vsteps,
+    scales,
     in_sem,
     x_sem,
     out_sem,
@@ -205,6 +199,10 @@
 
     small[2].wait()
     acc[...] = jnp.zeros_like(acc)
+    head = lax.broadcasted_iota(jnp.int32, (1, cv), 1) // VDIM
+    lam = jnp.zeros((1, cv), f32)
+    for h in range(cv // VDIM):
+        lam = jnp.where(head == h, lam_ref[h], lam)
     for c in range(CHUNKS):
         for copy in chunk_copies(c):
             copy.wait()
@@ -212,7 +210,6 @@
         def multiply(i, carry):
             at = pl.ds(pl.multiple_of(c * tokens + i * STEP_TOKENS, STEP_TOKENS), STEP_TOKENS)
             upper = jnp.dot(xv[at, :], pv[...], preferred_element_type=f32).astype(bf16)
-            lam = lam_ref[...]
             value = (fcv[at, :].astype(f32) - lam * scv[at, :].astype(f32)).astype(bf16)
             over = (((0,), (0,)), ((), ()))
             acc[:, :cg] += lax.dot_general(upper, gcv[at, :], over, preferred_element_type=f32)
@@ -261,7 +258,6 @@
 
     for k in range(1, nz):
         rz(k, z, zpeer(k)).start()
-    send_z(2)
     relay(1)
     for i in range(3, 7):
         small[i].wait()
@@ -286,10 +282,8 @@
                 (gs, ngs_hbm),
                 (vm, nvm_hbm),
                 (vs, nvs_hbm),
-                (gw, ngw_hbm),
-                (vw, nvw_hbm),
-                (gsteps, gstep_hbm),
-                (vsteps, vstep_hbm),
+                (direct, dir_hbm),
+                (scales, scale_hbm),
             ]
         )
     ]
@@ -322,8 +316,8 @@
         dz(k, z).start()
     for m in range(1, nx):
         dx(m, z, x).start()
+    send_z(2)
     send_z(3)
-    relay(2)
     for k in range(1, nz):
         dz(k, zpeer(k)).wait_recv()
         for m in range(1, nx):
@@ -332,14 +326,17 @@
         for zi in range(nz):
             dx(m, zi, xpeer(m)).wait_recv()
 
+    relay(2)
+    relay(3)
     for j in range(nfs):
         dcat[pl.ds(j * share, share), :] = dall[j].astype(f32)
     direction = dcat[...].astype(bf16)
+    direct[...] = direction
+    outs[4].start()
 
     def expand(j, squares):
         left = pv[pl.ds(pl.multiple_of(j * rows, rows), rows), :]
         block = jnp.dot(left, direction, preferred_element_type=f32)
-        upd[j] = block
         return squares + jnp.sum(block * block, axis=0, keepdims=True)
 
     squares = lax.fori_loop(0, nfs, expand, jnp.zeros((1, cols), f32))
@@ -360,41 +357,23 @@
 
     for k in range(1, nt):
         tp(k, t).start()
-    relay(3)
     for k in range(1, nt):
         tp(k, lax.rem(t + k, nt)).wait_recv()
     whole = sums[0]
     for k in range(1, nt):
         whole = whole + sums[k]
     entries = nfs * rows * nt
-    gscale = (1.0 / (jnp.sqrt(whole[0] / (entries * cg)) + rms_floor))[0:1, 0:1]
-    vscale = (1.0 / (jnp.sqrt(whole[1] / (entries * cv)) + rms_floor))[0:1, 0:1]
-
-    gstep = upd[f, :, :cg] * gscale
-    vstep = upd[f, :, cg:] * vscale
-    gsteps[...] = gstep
-    vsteps[...] = vstep
-    gw[...] = gw[...] - learn_rate * gstep
-    vw[...] = vw[...] - learn_rate * vstep
-    for i in range(4, 8):
-        outs[i].start()
+    scales[0] = 1.0 / (jnp.sqrt(whole[0] / (entries * cg)) + rms_floor)
+    scales[1] = 1.0 / (jnp.sqrt(whole[1] / (entries * cv)) + rms_floor)
+    outs[5].start()
 
     copies = []
     for p in range(PIECES):
         for m in range(1, nx):
             for zi in range(nz):
                 wx(m, p, zi, xpeer(m)).wait_recv()
-        at = pl.ds(p * part, part)
-
-        def finish(j, carry):
-            gcs[j, p] = (wall[j, p, :, :cg].astype(f32) - learn_rate * (upd[j, at, :cg] * gscale)).astype(bf16)
-            vcs[j, p] = (wall[j, p, :, cg:].astype(f32) - learn_rate * (upd[j, at, cg:] * vscale)).astype(bf16)
-            return carry
-
-        lax.fori_loop(0, nfs, finish, 0)
-        for i, (src, dst) in enumerate([(gcs, gcopy_hbm), (vcs, vcopy_hbm)]):
-            copies.append(pltpu.make_async_copy(src.at[:, p], dst.at[:, p], copy_sem.at[i, p]))
-            copies[-1].start()
+        copies.append(pltpu.make_async_copy(wall.at[:, p], wall_hbm.at[:, p], copy_sem.at[p]))
+        copies[-1].start()
 
     for copy in copies + outs:
         copy.wait()
@@ -413,6 +392,106 @@
         tp(k, t).wait_send()
 
 
+def finish_kernel(
+    nz,
+    nx,
+    proj_hbm,
+    gw_hbm,
+    vw_hbm,
+    wall,
+    dir_hbm,
+    scale_ref,
+    ngm_hbm,
+    ngs_hbm,
+    nvm_hbm,
+    nvs_hbm,
+    ngw_out,
+    gstep_out,
+    gcopy_out,
+    ngm_out,
+    ngs_out,
+    nvw_out,
+    vstep_out,
+    vcopy_out,
+    nvm_out,
+    nvs_out,
+    pv,
+    gw,
+    vw,
+    direct,
+    gm,
+    gs,
+    vm,
+    vs,
+    gcs,
+    vcs,
+    gsteps,
+    vsteps,
+    in_sem,
+    out_sem,
+    copy_sem,
+):
+    nfs = nz * nx
+    f = lax.axis_index("fs")
+    rows, cg = gw.shape
+    moments = [(ngm_hbm, gm, ngm_out), (ngs_hbm, gs, ngs_out), (nvm_hbm, vm, nvm_out), (nvs_hbm, vs, nvs_out)]
+    loads = [(dir_hbm, direct), (proj_hbm, pv), (gw_hbm, gw), (vw_hbm, vw)]
+    loads += [(src, held) for src, held, _ in moments]
+    loads = [pltpu.make_async_copy(src, dst, in_sem.at[i]) for i, (src, dst) in enumerate(loads)]
+    stores = [(held, dst) for _, held, dst in moments]
+    stores += [(gw, ngw_out), (vw, nvw_out), (gsteps, gstep_out), (vsteps, vstep_out)]
+    stores = [pltpu.make_async_copy(src, dst, out_sem.at[i]) for i, (src, dst) in enumerate(stores)]
+
+    def put(j):
+        return [
+            pltpu.make_async_copy(gcs.at[j], gcopy_out.at[j], copy_sem.at[0, j]),
+            pltpu.make_async_copy(vcs.at[j], vcopy_out.at[j], copy_sem.at[1, j]),
+        ]
+
+    for i in range(2):
+        loads[i].start()
+    for i in range(2, 8):
+        loads[i].start()
+    gscale = scale_ref[0, 0:1, 0:1]
+    vscale = scale_ref[1, 0:1, 0:1]
+    for i in range(2):
+        loads[i].wait()
+    direction = direct[...]
+
+    def block(j):
+        left = pv[pl.ds(pl.multiple_of(j * rows, rows), rows), :]
+        return jnp.dot(left, direction, preferred_element_type=f32)
+
+    def finish(j, carry):
+        update = block(j)
+        held = wall[j].astype(f32).reshape(update.shape)
+        gcs[j] = (held[:, :cg] - learn_rate * (update[:, :cg] * gscale)).astype(bf16)
+        vcs[j] = (held[:, cg:] - learn_rate * (update[:, cg:] * vscale)).astype(bf16)
+        for copy in put(j):
+            copy.start()
+        return carry
+
+    lax.fori_loop(0, nfs, finish, 0)
+    for i in range(2, 8):
+        loads[i].wait()
+    for i in range(4):
+        stores[i].start()
+    mine = block(f)
+    gstep = mine[:, :cg] * gscale
+    vstep = mine[:, cg:] * vscale
+    gsteps[...] = gstep
+    vsteps[...] = vstep
+    gw[...] = gw[...] - learn_rate * gstep
+    vw[...] = vw[...] - learn_rate * vstep
+    for i in range(4, 8):
+        stores[i].start()
+    for j in range(nfs):
+        for copy in put(j):
+            copy.wait()
+    for copy in stores:
+        copy.wait()
+
+
 def per_device(nz, nx, nt, xin, gcot, fcot, scot, lam, proj, gw, gm, gs, vw, vm, vs):
     nfs = nz * nx
     rows, cg = gw.shape
@@ -421,39 +500,37 @@
     depth, rank = proj.shape
     share = rank // nfs
     part = rows // PIECES
-    column_lambda = jnp.repeat(lam, VDIM)[None, :]
     anywhere = pl.BlockSpec(memory_space=pl.ANY)
+    pinned = pl.BlockSpec(memory_space=pl.ANY)
     dma = pltpu.SemaphoreType.DMA
     shape = jax.ShapeDtypeStruct
     like = lambda a: shape(a.shape, a.dtype)
-    results = pl.pallas_call(
+    vmem = lambda a: pltpu.VMEM(a.shape, a.dtype)
+    wall, direction, scale, *moments = pl.pallas_call(
         functools.partial(kernel, nz, nx, nt),
         out_shape=[
-            like(gw),
-            like(gw),
-            shape((nfs, PIECES, part, cg), bf16),
+            shape((nfs, PIECES, part, cols), bf16),
+            shape((rank, cols), bf16),
+            shape((2, 8, 128), f32),
             like(gm),
             like(gs),
-            like(vw),
-            like(vw),
-            shape((nfs, PIECES, part, cv), bf16),
             like(vm),
             like(vs),
         ],
-        in_specs=[anywhere] * 4 + [pl.BlockSpec(memory_space=pltpu.VMEM)] + [anywhere] * 7,
-        out_specs=[anywhere] * 10,
+        in_specs=[pinned] * 4 + [pl.BlockSpec(memory_space=pltpu.SMEM)] + [pinned] * 7,
+        out_specs=[anywhere] * 7,
         scratch_shapes=[
-            pltpu.VMEM(xin.shape, bf16),
-            pltpu.VMEM(gcot.shape, bf16),
-            pltpu.VMEM(fcot.shape, bf16),
-            pltpu.VMEM(scot.shape, bf16),
-            pltpu.VMEM(proj.shape, bf16),
-            pltpu.VMEM(gw.shape, f32),
-            pltpu.VMEM(vw.shape, f32),
-            pltpu.VMEM(gm.shape, f32),
-            pltpu.VMEM(gs.shape, f32),
-            pltpu.VMEM(vm.shape, f32),
-            pltpu.VMEM(vs.shape, f32),
+            vmem(xin),
+            vmem(gcot),
+            vmem(fcot),
+            vmem(scot),
+            vmem(proj),
+            vmem(gw),
+            vmem(vw),
+            vmem(gm),
+            vmem(gs),
+            vmem(vm),
+            vmem(vs),
             pltpu.VMEM((nfs, PIECES, part, cols), bf16),
             pltpu.VMEM((rank, cols), f32),
             pltpu.VMEM((nx, nz, share, cols), bf16),
@@ -462,16 +539,13 @@
             pltpu.VMEM((nz, share, cols), bf16),
             pltpu.VMEM((nfs, share, cols), bf16),
             pltpu.VMEM((rank, cols), f32),
-            pltpu.VMEM((nfs, rows, cols), f32),
+            pltpu.VMEM((rank, cols), bf16),
             pltpu.VMEM((nt, 2, 8, 128), f32),
-            pltpu.VMEM((nfs, PIECES, part, cg), bf16),
-            pltpu.VMEM((nfs, PIECES, part, cv), bf16),
-            pltpu.VMEM(gw.shape, f32),
-            pltpu.VMEM(vw.shape, f32),
+            pltpu.VMEM((2, 8, 128), f32),
             dma((7,)),
             dma((4, CHUNKS)),
-            dma((8,)),
-            dma((2, PIECES)),
+            dma((6,)),
+            dma((PIECES,)),
             dma((nz, PIECES)),
             dma((nz, PIECES)),
             dma((nx, nz, PIECES)),
@@ -490,7 +564,42 @@
         compiler_params=pltpu.CompilerParams(
             collective_id=0, has_side_effects=True, vmem_limit_bytes=60 * 1024 * 1024
         ),
-    )(xin, gcot, fcot, scot, column_lambda, proj, gw, gm, gs, vw, vm, vs)
+    )(xin, gcot, fcot, scot, lam, proj, gw, gm, gs, vw, vm, vs)
+    results = pl.pallas_call(
+        functools.partial(finish_kernel, nz, nx),
+        out_shape=[
+            like(gw),
+            like(gw),
+            shape((nfs, rows, cg), bf16),
+            like(gm),
+            like(gs),
+            like(vw),
+            like(vw),
+            shape((nfs, rows, cv), bf16),
+            like(vm),
+            like(vs),
+        ],
+        in_specs=[pinned] * 3 + [pl.BlockSpec(memory_space=pltpu.VMEM), anywhere] + [pl.BlockSpec(memory_space=pltpu.VMEM)] + [anywhere] * 4,
+        out_specs=[anywhere] * 10,
+        scratch_shapes=[
+            vmem(proj),
+            vmem(gw),
+            vmem(vw),
+            vmem(direction),
+            vmem(gm),
+            vmem(gs),
+            vmem(vm),
+            vmem(vs),
+            pltpu.VMEM((nfs, rows, cg), bf16),
+            pltpu.VMEM((nfs, rows, cv), bf16),
+            vmem(gw),
+            vmem(vw),
+            dma((8,)),
+            dma((8,)),
+            dma((2, nfs)),
+        ],
+        compiler_params=pltpu.CompilerParams(vmem_limit_bytes=60 * 1024 * 1024),
+    )(proj, gw, vw, wall, direction, scale, *moments)
     results = list(results)
     results[2] = results[2].reshape(depth, cg)
     results[7] = results[7].reshape(depth, cv)

time: 77.3 us -> 69.3 us (0.90)
  local copies, waits for them, and re-layouts: 11.4 us -> 0 us
  Pallas kernels: 65 us -> 68.5 us
    unnamed x26 -> x0, local copies, waits for them, and re-layouts: 10.1 us -> none
    pallas_call x1 -> x2, Pallas kernels: 65 us -> 68.5 us  [the longest x1 61.1 us: per_device(): pl.pallas_call(functools.partial(kernel, nz, nx, nt), out_shape=[shape((n...]
    broadcast_in_dim x1 -> x0, local copies, waits for them, and re-layouts: 1.29 us -> none  [per_device(): column_lambda = jnp.repeat(lam, VDIM)[None, :]]
where the time goes in v2:
time: 69.3 us; the launch traced here: 69.1 us
  Pallas kernels  68.5 us (99%)
    pallas_call x1, Pallas kernels, per_device(): pl.pallas_call(functools.partial(kernel, nz, nx, nt), out_shape=[shape((n...  61.1 us
    pallas_call x1, Pallas kernels, per_device(): pl.pallas_call(functools.partial(finish_kernel, nz, nx), out_shape=[like(...  7.37 us

profile of v2, /device:TPU:12, one launch (start us, length us, event | category | flops | bytes accessed | tf_op | source)
XLA Modules:
  0.0 69.1 jit_solution(14173665450648370555)
XLA Ops:
  0.6 61.1 %shard_map.195 = (bf16[8,4,64,768]{3,2,1,0:T(8,128)(2,1)}, bf16[256,768]{1,0:T(8,128)(2,1)}, f32[2,8,128]{2,1,0:T(8,128)}, f32[32,512]{1,0:T(8,128)}, f32[32,512...) custom-call(bf16[2048,2048]{1,0:T(8,128)(2,1)} %x_hbm.1, bf16[2048,512]{1,0:T(8,128)(2,1)} %gcot_hbm.1, ...), custom_call_target="tpu_custom_call" | custom-call | tf_op jit(solution)/shard_map/pallas_call | solution.py:509
  61.8 7.4 %shard_map.196 = (f32[256,512]{1,0:T(8,128)}, f32[256,512]{1,0:T(8,128)}, bf16[8,256,512]{2,1,0:T(8,128)(2,1)}, f32[32,512]{1,0:T(8,128)}, f32[32,512]{1,0:T(8,1...) custom-call(bf16[2048,256]{1,0:T(8,128)(2,1)} %proj_hbm.3, ...), custom_call_target="tpu_custom_call" | custom-call | tf_op jit(solution)/shard_map/pallas_call | solution.py:568
